TPU v7x, 32 devices: a whole 2x2x4 slice. The times are simulated.
32 devices in a mesh: grp: 2 (over y), sp: 4 (over z), tp: 4 (over x, core).
Axes of the slice: x: 2, y: 2, z: 4, core: 2. Of those that a mesh axis runs over, the one named last changes fastest.
Arguments:
- queries: bfloat16 [4096, 1024], P(('grp', 'sp'), 'tp'), parts along dimension 0, may hold values from -120 to 120
- keys: bfloat16 [4096, 256], P(('grp', 'sp')), parts along dimension 0, may hold values from -6 to 6
- values: bfloat16 [4096, 256], P(('grp', 'sp')), parts along dimension 0, may hold values from -6 to 6
- sink: float32 [8], P('tp'), may hold values from 1 to 5
- resid: bfloat16 [4096, 2048], P(('grp', 'sp')), parts along dimension 0, may hold values from -100 to 100
- out_proj: bfloat16 [1024, 2048], P(None, 'tp'), may hold values from -1.5 to 1.5
- norm_gain: float32 [2048], replicated, may hold values from 0.1 to 1.9
- w_gate: bfloat16 [2048, 6144], P('sp', 'tp'), may hold values from -0.125 to 0.125
- w_up: bfloat16 [2048, 6144], P('sp', 'tp'), may hold values from -0.125 to 0.125
- conv_w: float32 [3, 6144], P(None, 'tp'), may hold values from -3 to 3
- conv_b: float32 [6144], P('tp'), may hold values from -3 to 3
- w_down: bfloat16 [6144, 2048], P('tp', 'sp'), may hold values from -0.21875 to 0.21875
Outputs:
- layer_out: bfloat16 [4096, 2048], P(('grp', 'sp'), 'tp'), parts along dimension 0
There are 2 independent parts, one for each index of `grp`. A program takes and returns all parts, laid end to end along the dimension named above; an argument that names none is the same for every part. Nothing has to cross between parts.
All inputs are finite; a program needn't handle non-finite values.
Results may differ from a plain program's by a relative error of at most 0.015.
Values may be sent and summed in bfloat16 or wider, within the bound.
A program may use at most 64 MiB of HBM per device.

v0:
```python
import jax
import jax.numpy as jnp
from jax import lax
from jax.sharding import PartitionSpec as P

H = 8
KVH = 2
HD = 128
WINDOW = 128
CONV = 3


def with_halo(cells, sides, width):
    for axis, dim in sides:
        count = lax.axis_size(axis)
        ends = count - 1
        head = lax.slice_in_dim(cells, 0, width, axis=dim)
        tail = lax.slice_in_dim(cells, cells.shape[dim] - width, cells.shape[dim], axis=dim)
        cells = jnp.concatenate(
            [
                lax.ppermute(tail, axis, [(i, (i + 1) % count) for i in range(ends)]),
                cells,
                lax.ppermute(head, axis, [((i + 1) % count, i) for i in range(ends)]),
            ],
            axis=dim,
        )
    return cells


def shards(
    queries, keys, values, sink, resid, out_proj, norm_gain, w_gate, w_up, conv_w, conv_b, w_down
):
    tokens = queries.shape[0]
    width = resid.shape[1]
    heads_here = sink.shape[0]
    group = H // KVH
    scale = HD ** (-0.5)
    first_head = lax.axis_index("tp") * heads_here
    kv_head = first_head // group
    own_keys = lax.dynamic_slice_in_dim(keys, kv_head * HD, HD, 1)
    own_values = lax.dynamic_slice_in_dim(values, kv_head * HD, HD, 1)
    extended = with_halo(jnp.stack([own_keys, own_values]), (("sp", 1),), WINDOW)
    ext_keys = extended[0]
    ext_values = extended[1]
    span = tokens + 2 * WINDOW
    q_heads = queries.reshape(tokens, heads_here, HD)
    scores = (
        jnp.einsum("qhd,kd->hqk", q_heads, ext_keys, preferred_element_type=jnp.float32) * scale
    )
    offset = lax.axis_index("sp") * tokens
    q_pos = offset + jnp.arange(tokens, dtype=jnp.int32)[:, None]
    k_pos = offset - WINDOW + jnp.arange(span, dtype=jnp.int32)[None, :]
    seq_total = tokens * lax.axis_size("sp")
    valid = (jnp.abs(q_pos - k_pos) <= WINDOW) & (k_pos >= 0) & (k_pos < seq_total)
    scores = jnp.where(valid[None], scores, jnp.float32(-1e30))
    sink_col = sink[:, None]
    top = jnp.maximum(jnp.max(scores, axis=-1), sink_col)
    expo = jnp.exp(scores - top[..., None])
    total = jnp.sum(expo, axis=-1) + jnp.exp(sink_col - top)
    weights = (expo / total[..., None]).astype(jnp.bfloat16)
    heads_out = jnp.einsum("hqk,kd->qhd", weights, ext_values, preferred_element_type=jnp.float32)
    heads_out = heads_out.astype(jnp.bfloat16).reshape(tokens, heads_here * HD)
    all_heads = lax.all_gather(heads_out, "tp", axis=1, tiled=True)
    cols = width // lax.axis_size("tp")
    col_start = lax.axis_index("tp") * cols
    full_proj = lax.all_gather(out_proj, "tp", axis=1, tiled=True)
    summed = resid.astype(jnp.float32) + jnp.dot(
        all_heads, full_proj, preferred_element_type=jnp.float32
    )
    mean = jnp.mean(summed, axis=-1, keepdims=True)
    msq = jnp.mean(summed * summed, axis=-1, keepdims=True)
    normed_full = ((summed - mean) * lax.rsqrt(msq - mean * mean + 1e-05) * norm_gain).astype(
        jnp.bfloat16
    )
    normed_own = lax.dynamic_slice_in_dim(normed_full, col_start, cols, 1)
    gate_acc = jnp.dot(
        normed_full,
        lax.all_gather(w_gate, "sp", axis=0, tiled=True),
        preferred_element_type=jnp.float32,
    )
    up_acc = jnp.dot(
        normed_full,
        lax.all_gather(w_up, "sp", axis=0, tiled=True),
        preferred_element_type=jnp.float32,
    )
    gate_pre = gate_acc.astype(jnp.bfloat16)
    up_part = up_acc.astype(jnp.bfloat16)
    padded = with_halo(gate_pre, (("sp", 0),), CONV // 2)
    conv = conv_b
    for tap in range(CONV):
        conv = conv + padded[tap : tap + tokens].astype(jnp.float32) * conv_w[tap]
    act = (jax.nn.silu(conv) * up_part.astype(jnp.float32)).astype(jnp.bfloat16)
    terms = jnp.dot(
        act, lax.all_gather(w_down, "sp", axis=1, tiled=True), preferred_element_type=jnp.float32
    )
    ffn_own = lax.psum_scatter(
        terms.astype(jnp.bfloat16), "tp", scatter_dimension=1, tiled=True
    ).astype(jnp.float32)
    return (normed_own.astype(jnp.float32) + ffn_own).astype(jnp.bfloat16)


def solution(mesh):
    return jax.shard_map(
        shards,
        mesh=mesh,
        in_specs=(
            P(("grp", "sp"), "tp"),
            P(("grp", "sp"), None),
            P(("grp", "sp"), None),
            P("tp"),
            P(("grp", "sp"), None),
            P(None, "tp"),
            P(),
            P("sp", "tp"),
            P("sp", "tp"),
            P(None, "tp"),
            P("tp"),
            P("tp", "sp"),
        ),
        out_specs=P(("grp", "sp"), "tp"),
        check_vma=False,
    )
```

profile of v0, /device:TPU:0, one launch (start us, length us, event | category | flops | bytes accessed | tf_op | source)
XLA Modules:
  0.0 476.0 jit_solution(9016852230966235995)
XLA Ops:
  6.5 1.0 dynamic-slice_bitcast_fusion
  7.6 5.0 %collective-permute-start = (bf16[2,128,128]{2,1,0:T(8,128)(2,1)S(1)}, bf16[2,128,128]{2,1,0:T(8,128)(2,1)S(1)}, u32[]{:S(2)}, u32[]{:S(2)}) collective-permute-start(bf16[2,128,128]{2,1,0:T(8,128)(2,1)S(1)} %get-tuple-element.12), channel_id=1, source_target_pairs={{0,4},{4,8},{8,12},{1,5},{5,9},{9,13},{2,6},{6,10},{10,14},{3,7},{... | collective-permute-start | bytes 196616 | tf_op jit(solution)/shard_map/ppermute | solution.py:21
  12.6 1.3 collective-permute-start.1
  13.9 0.8 fusion.10
  14.7 4.0 collective-permute-done.1
  18.8 0.8 fusion.1
  19.6 0.7 fusion
  20.4 1.9 fusion.12
  22.3 0.7 all-gather.8.cloned.1.call-update
  23.1 0.7 all-gather.10.cloned.1.call-update
  24.4 0.5 all-gather.14.cloned.1.call-update
  25.0 14.4 %all-gather.6.cloned.1.call-done = bf16[512,1024]{0,1:T(8,128)(2,1)} async-done(((bf16[512,256]{0,1:T(8,128)(2,1)}), bf16[512,1024]{0,1:T(8,128)(2,1)}) %all-gather.6.cloned.1.call-update) | async-done | bytes 1048592 | tf_op jit(solution)/shard_map/all_gather | solution.py:63
  39.4 36.0 %all-gather.8.cloned.1.call-done = bf16[1024,2048]{1,0:T(8,128)(2,1)} async-done(((bf16[1024,512]{1,0:T(8,128)(2,1)}), bf16[1024,2048]{1,0:T(8,128)(2,1)}) %all-gather.8.cloned.1.call-update) | async-done | bytes 4194320 | tf_op jit(solution)/shard_map/all_gather | solution.py:66
  75.4 5.4 %fusion.22 = (f32[512]{0:T(512)S(1)}, f32[512]{0:T(512)S(1)}, f32[512,2048]{1,0:T(8,128)S(1)}) fusion(bf16[512,1024]{0,1:T(8,128)(2,1)} %all-gather.6.cloned.1.call-done, bf16[1024,2048]{1,0:T(8,128)(2,1)} %all-gather.8.cloned.1.call-done, bf16[512,2048]{1,0:T(8,128)(2,1)S(1)} %copy-done.5), kind=kOutput, calls=%fused_computation.52 | convolution fusion | flops 2152725504 | bytes 11538432 | tf_op jit(solution)/shard_map/dot_general | solution.py:67
  80.8 0.6 multiply_convert_fusion
  81.5 110.9 %all-gather.10.cloned.1.call-done = bf16[2048,1536]{1,0:T(8,128)(2,1)} async-done(((bf16[512,1536]{1,0:T(8,128)(2,1)}), bf16[2048,1536]{1,0:T(8,128)(2,1)}) %all-gather.10.cloned.1.call-update) | async-done | bytes 6291472 | tf_op jit(solution)/shard_map/all_gather | solution.py:78
  192.4 6.2 %convolution_convert_fusion.2 = bf16[512,1536]{1,0:T(8,128)(2,1)S(1)} fusion(bf16[512,2048]{1,0:T(8,128)(2,1)S(1)} %multiply_convert_fusion, bf16[2048,1536]{1,0:T(8,128)(2,1)} %all-gather.10.cloned.1.call-done), kind=kOutput, calls=%fused_computation.9 | convolution fusion | flops 3222011904 | bytes 9961472 | tf_op jit(solution)/shard_map/dot_general | solution.py:76
  198.6 1.3 collective-permute-start.2
  199.9 1.5 collective-permute-start.3
  201.5 105.9 %all-gather.12.cloned.1.call-done = bf16[2048,1536]{1,0:T(8,128)(2,1)} async-done(((bf16[512,1536]{1,0:T(8,128)(2,1)}), bf16[2048,1536]{1,0:T(8,128)(2,1)}) %all-gather.12.cloned.1.call-update) | async-done | bytes 6291472 | tf_op jit(solution)/shard_map/all_gather | solution.py:83
  307.4 114.9 %all-gather.14.cloned.1.call-done = bf16[1536,2048]{1,0:T(8,128)(2,1)} async-done(((bf16[1536,512]{1,0:T(8,128)(2,1)}), bf16[1536,2048]{1,0:T(8,128)(2,1)}) %all-gather.14.cloned.1.call-update) | async-done | bytes 6291472 | tf_op jit(solution)/shard_map/all_gather | solution.py:94
  422.3 15.3 %convolution_convert_fusion = bf16[512,2048]{1,0:T(8,128)(2,1)} fusion(bf16[1536,2048]{1,0:T(8,128)(2,1)} %all-gather.14.cloned.1.call-done, bf16[512,1536]{1,0:T(8,128)(2,1)} %copy-done.4, bf16[1,1536]{1,0:T(2,128)(2,1)S(1)} %collective-permute-done.3, bf16[1,1536]{1,0:T(2,128)(2,1)S(1)} %collective-permute-done.2, f32[1536]{0:T(1024)S(1)} %get-tuple-element.8, ...), kind=kOutput, calls=%fused_computation.7 | convolution fusion | flops 6461587456 | bytes 18380800 | tf_op jit(solution)/shard_map/dot_general | solution.py:93
  437.6 29.5 %reduce-scatter.2.cloned.1.call-done = bf16[512,512]{1,0:T(8,128)(2,1)} async-done(((bf16[512,2048]{1,0:T(8,128)(2,1)}), bf16[512,512]{1,0:T(8,128)(2,1)}) %reduce-scatter.2.cloned.1.call-update) | async-done | bytes 524304 | tf_op jit(solution)/shard_map/reduce_scatter | solution.py:96
  467.1 2.0 add_convert_fusion
  (36 shorter events, 1.1 us)
Async XLA Ops:
  6.5 12.2 %copy-start = (bf16[512,256]{1,0:T(8,128)(2,1)S(1)}, bf16[512,256]{1,0:T(8,128)(2,1)}, u32[]{:S(2)}) copy-start(bf16[512,256]{1,0:T(8,128)(2,1)} %param.12) | copy-start | bytes 786436
  6.5 32.8 %all-gather.6.cloned.1.call-start = ((), (), s32[]{:S(2)}) async-start(), calls=%async_computation.1 | async-start | bytes 1310720 | tf_op jit(solution)/shard_map/all_gather | solution.py:63
  6.5 13.0 %copy-start.3 = (f32[2]{0:T(128)S(1)}, f32[2]{0:T(128)}, u32[]{:S(2)}) copy-start(f32[2]{0:T(128)} %param.15) | copy-start | bytes 28
  7.6 7.1 %collective-permute-start = (bf16[2,128,128]{2,1,0:T(8,128)(2,1)S(1)}, bf16[2,128,128]{2,1,0:T(8,128)(2,1)S(1)}, u32[]{:S(2)}, u32[]{:S(2)}) collective-permute-start(bf16[2,128,128]{2,1,0:T(8,128)(2,1)S(1)} %get-tuple-element.12), channel_id=1, source_target_pairs={{0,4},{4,8},{8,12},{1,5},{5,9},{9,13},{2,6},{6,10},{10,14},{3,7},{... | collective-permute-start | bytes 196616 | tf_op jit(solution)/shard_map/ppermute | solution.py:21
  12.6 6.2 %collective-permute-start.1 = (bf16[2,128,128]{2,1,0:T(8,128)(2,1)S(1)}, bf16[2,128,128]{2,1,0:T(8,128)(2,1)S(1)}, u32[]{:S(2)}, u32[]{:S(2)}) collective-permute-start(bf16[2,128,128]{2,1,0:T(8,128)(2,1)S(1)} %get-tuple-element.13), channel_id=1, source_target_pairs={{4,0},{8,4},{12,8},{5,1},{9,5},{13,9},{6,2},{10,6},{14,10},{7,3},{... | collective-permute-start | bytes 196616 | tf_op jit(solution)/shard_map/ppermute | solution.py:23
  22.3 53.2 %copy-start.5 = (bf16[512,2048]{1,0:T(8,128)(2,1)S(1)}, bf16[512,2048]{1,0:T(8,128)(2,1)}, u32[]{:S(2)}) copy-start(bf16[512,2048]{1,0:T(8,128)(2,1)} %param.16) | copy-start | bytes 6291460
  22.3 53.1 %all-gather.8.cloned.1.call-start = ((), (), s32[]{:S(2)}) async-start(), calls=%async_computation.2 | async-start | bytes 5242880 | tf_op jit(solution)/shard_map/all_gather | solution.py:66
  23.1 169.3 %all-gather.10.cloned.1.call-start = ((), (), s32[]{:S(2)}) async-start(), calls=%async_computation.3 | async-start | bytes 7864320 | tf_op jit(solution)/shard_map/all_gather | solution.py:78
  23.8 283.6 %all-gather.12.cloned.1.call-start = ((), (), s32[]{:S(2)}) async-start(), calls=%async_computation.4 | async-start | bytes 7864320 | tf_op jit(solution)/shard_map/all_gather | solution.py:83
  24.4 398.0 %all-gather.14.cloned.1.call-start = ((), (), s32[]{:S(2)}) async-start(), calls=%async_computation.5 | async-start | bytes 7864320 | tf_op jit(solution)/shard_map/all_gather | solution.py:94
  24.9 55.9 %copy-start.2 = (f32[2048]{0:T(1024)S(1)}, f32[2048]{0:T(1024)}, u32[]{:S(2)}) copy-start(f32[2048]{0:T(1024)} %param.18) | copy-start | bytes 24580
  25.0 442.2 %reduce-scatter.2.cloned.1.call-start = ((), (), s32[]{:S(2)}) async-start(), calls=%async_computation.6 | async-start | bytes 2621440 | tf_op jit(solution)/shard_map/reduce_scatter | solution.py:96
  81.5 119.9 %copy-start.1 = (f32[3,1536]{1,0:T(4,128)S(1)}, f32[3,1536]{1,0:T(4,128)}, u32[]{:S(2)}) copy-start(f32[3,1536]{1,0:T(4,128)} %param.21) | copy-start | bytes 55300
  81.5 340.9 %copy-start.6 = (f32[1536]{0:T(1024)S(1)}, f32[1536]{0:T(1024)}, u32[]{:S(2)}) copy-start(f32[1536]{0:T(1024)} %param.22) | copy-start | bytes 18436
  198.6 2.8 copy-start.4
  198.6 223.7 %collective-permute-start.2 = (bf16[1,1536]{1,0:T(2,128)(2,1)S(1)}, bf16[1,1536]{1,0:T(2,128)(2,1)S(1)}, u32[]{:S(2)}, u32[]{:S(2)}) collective-permute-start(bf16[1,1536]{1,0:T(2,128)(2,1)S(1)} %get-tuple-element.10), channel_id=1, source_target_pairs={{0,4},{4,8},{8,12},{1,5},{5,9},{9,13},{2,6},{6,10},{10,14},{3,7},{... | collective-permute-start | bytes 9224 | tf_op jit(solution)/shard_map/ppermute | solution.py:21
  199.9 222.4 %collective-permute-start.3 = (bf16[1,1536]{1,0:T(2,128)(2,1)S(1)}, bf16[1,1536]{1,0:T(2,128)(2,1)S(1)}, u32[]{:S(2)}, u32[]{:S(2)}) collective-permute-start(bf16[1,1536]{1,0:T(2,128)(2,1)S(1)} %get-tuple-element.11), channel_id=1, source_target_pairs={{4,0},{8,4},{12,8},{5,1},{9,5},{13,9},{6,2},{10,6},{14,10},{7,3},{... | collective-permute-start | bytes 9224 | tf_op jit(solution)/shard_map/ppermute | solution.py:23
Sparse Core Ops, SparseCore 0:
  22.4 16.9 all-gather.5
  40.9 34.4 all-gather.7
  77.0 115.3 all-gather.9
  193.8 113.5 all-gather.11
  308.8 113.4 all-gather.13
  437.7 29.3 reduce-scatter.1
where the time goes:
time: 476 us
  waiting for transfers between devices  418 us (88%)
  matrix products  29.4 us (6%)
  between operations  13.7 us (3%)
  starting transfers between devices  9.21 us (2%)
    all_gather x1, waiting for transfers between devices, shards(): lax.all_gather(w_down, 'sp', axis=1, tiled=True)  115 us
    all_gather x1, waiting for transfers between devices, shards(): lax.all_gather(w_gate, 'sp', axis=0, tiled=True)  111 us
    all_gather x1, waiting for transfers between devices, shards(): lax.all_gather(w_up, 'sp', axis=0, tiled=True)  106 us
    all_gather x1, waiting for transfers between devices, shards(): full_proj = lax.all_gather(out_proj, 'tp', axis=1, tiled=True)  36 us
    reduce_scatter x1, waiting for transfers between devices, shards(): lax.psum_scatter(terms.astype(jnp.bfloat16), 'tp', scatter_dimension=1, t...  29.5 us
    dot_general x1, matrix products, shards(): jnp.dot(act, lax.all_gather(w_down, 'sp', axis=1, tiled=True), preferred_...  15.3 us
    all_gather x1, waiting for transfers between devices, shards(): all_heads = lax.all_gather(heads_out, 'tp', axis=1, tiled=True)  14.4 us
  transfers between devices with their start and end apart: 10, of which 7 were waited for; matrix products, arithmetic and copies ran while one was open for 3% of the time, Pallas kernels for 0%

commit v1 on v0

--- a/solution.py
+++ b/solution.py
@@ -63,7 +63,12 @@
     all_heads = lax.all_gather(heads_out, "tp", axis=1, tiled=True)
     cols = width // lax.axis_size("tp")
     col_start = lax.axis_index("tp") * cols
-    full_proj = lax.all_gather(out_proj, "tp", axis=1, tiled=True)
+    ring = [out_proj]
+    for hop in range(3):
+        ring.append(lax.ppermute(ring[-1], "tp", [(dev, (dev + 1) % 4) for dev in range(4)]))
+    full_proj = jnp.roll(
+        jnp.concatenate(ring[::-1], axis=1), (lax.axis_index("tp") + 1) * ring[0].shape[1], axis=1
+    )
     summed = resid.astype(jnp.float32) + jnp.dot(
         all_heads, full_proj, preferred_element_type=jnp.float32
     )

time: 476 us -> 443 us (0.931)
  waiting for transfers between devices: 418 us -> 373 us
  local copies, waits for them, and re-layouts: 1.13 us -> 12.5 us
    ppermute x0 -> x3, waiting for transfers between devices: none -> 48.4 us  [shards(): lax.ppermute(ring[-1], 'tp', [(dev, (dev + 1) % 4) for dev in range(4)])]
    all_gather x1, waiting for transfers between devices: 111 us -> 68.2 us  [shards(): lax.all_gather(w_gate, 'sp', axis=0, tiled=True)]
    all_gather x1 -> x0, waiting for transfers between devices: 36 us -> none  [shards(): full_proj = lax.all_gather(out_proj, 'tp', axis=1, tiled=True)]
    all_gather x1, waiting for transfers between devices: 14.4 us -> 0.01 us  [shards(): all_heads = lax.all_gather(heads_out, 'tp', axis=1, tiled=True)]
    unnamed x14 -> x21, local copies, waits for them, and re-layouts: 0.03 us -> 10.3 us
    all_gather x1, waiting for transfers between devices: 106 us -> 115 us  [shards(): lax.all_gather(w_up, 'sp', axis=0, tiled=True)]
    all_gather x1, waiting for transfers between devices: 115 us -> 106 us  [shards(): lax.all_gather(w_down, 'sp', axis=1, tiled=True)]
  transfers between devices with their start and end apart: 10 -> 12, of which waited for: 7 -> 8; matrix products, arithmetic and copies ran while one was open for 3% -> 6% of each run, Pallas kernels for 0% -> 0%
where the time goes in v1:
time: 443 us
  waiting for transfers between devices  373 us (84%)
  matrix products  30.2 us (7%)
  between operations  13.4 us (3%)
  local copies, waits for them, and re-layouts  12.5 us (3%)
  starting transfers between devices  9.23 us (2%)
    all_gather x1, waiting for transfers between devices, shards(): lax.all_gather(w_up, 'sp', axis=0, tiled=True)  115 us
    all_gather x1, waiting for transfers between devices, shards(): lax.all_gather(w_down, 'sp', axis=1, tiled=True)  106 us
    all_gather x1, waiting for transfers between devices, shards(): lax.all_gather(w_gate, 'sp', axis=0, tiled=True)  68.2 us
    ppermute x3, waiting for transfers between devices, shards(): lax.ppermute(ring[-1], 'tp', [(dev, (dev + 1) % 4) for dev in range(4)])  48.4 us
    reduce_scatter x1, waiting for transfers between devices, shards(): lax.psum_scatter(terms.astype(jnp.bfloat16), 'tp', scatter_dimension=1, t...  29.5 us
    dot_general x1, matrix products, shards(): jnp.dot(act, lax.all_gather(w_down, 'sp', axis=1, tiled=True), preferred_...  15.3 us
    unnamed x21, local copies, waits for them, and re-layouts  10.3 us
  transfers between devices with their start and end apart: 12, of which 8 were waited for; matrix products, arithmetic and copies ran while one was open for 6% of the time, Pallas kernels for 0%

profile of v1, /device:TPU:0, one launch (start us, length us, event | category | flops | bytes accessed | tf_op | source)
XLA Modules:
  0.0 442.8 jit_solution(9426897391186587267)
XLA Ops:
  7.6 5.0 %collective-permute-start = (bf16[2,128,128]{2,1,0:T(8,128)(2,1)S(1)}, bf16[2,128,128]{2,1,0:T(8,128)(2,1)S(1)}, u32[]{:S(2)}, u32[]{:S(2)}) collective-permute-start(bf16[2,128,128]{2,1,0:T(8,128)(2,1)S(1)} %get-tuple-element.12), channel_id=1, source_target_pairs={{0,4},{4,8},{8,12},{1,5},{5,9},{9,13},{2,6},{6,10},{10,14},{3,7},{... | collective-permute-start | bytes 196616 | tf_op jit(solution)/shard_map/ppermute | solution.py:21
  12.6 1.3 collective-permute-start.1
  14.7 4.0 collective-permute-done.1
  20.4 1.9 fusion.16
  24.5 19.8 %collective-permute-done.2 = bf16[1024,512]{1,0:T(8,128)(2,1)S(1)} collective-permute-done((bf16[1024,512]{1,0:T(8,128)(2,1)S(1)}, bf16[1024,512]{1,0:T(8,128)(2,1)S(1)}, u32[]{:S(2)}, u32[]{:S(2)}) %collective-permute-start.2) | collective-permute-done | bytes 1048608 | tf_op jit(solution)/shard_map/ppermute | solution.py:68
  44.3 14.2 %collective-permute-done.3 = bf16[1024,512]{1,0:T(8,128)(2,1)S(1)} collective-permute-done((bf16[1024,512]{1,0:T(8,128)(2,1)S(1)}, bf16[1024,512]{1,0:T(8,128)(2,1)S(1)}, u32[]{:S(2)}, u32[]{:S(2)}) %collective-permute-start.3) | collective-permute-done | bytes 1048608 | tf_op jit(solution)/shard_map/ppermute | solution.py:68
  58.5 14.3 %collective-permute-done.4 = bf16[1024,512]{1,0:T(8,128)(2,1)} collective-permute-done((bf16[1024,512]{1,0:T(8,128)(2,1)S(1)}, bf16[1024,512]{1,0:T(8,128)(2,1)}, u32[]{:S(2)}, u32[]{:S(2)}) %collective-permute-start.4) | collective-permute-done | bytes 1048608 | tf_op jit(solution)/shard_map/ppermute | solution.py:68
  72.9 2.4 constant_dynamic-update-slice_fusion.7
  76.3 1.1 constant_dynamic-update-slice_fusion.5
  77.4 1.1 constant_dynamic-update-slice_fusion.4
  78.5 2.4 constant_dynamic-update-slice_fusion.3
  80.9 1.1 constant_dynamic-update-slice_fusion.2
  82.0 1.1 constant_dynamic-update-slice_fusion.1
  83.1 1.1 constant_dynamic-update-slice_fusion
  84.3 6.1 %fusion.27 = (f32[512]{0:T(512)S(1)}, f32[512]{0:T(512)S(1)}, f32[512,2048]{1,0:T(8,128)S(1)}) fusion(bf16[512,1024]{0,1:T(8,128)(2,1)} %all-gather.5.cloned.1.call-done, bf16[1024,4096]{1,0:T(8,128)(2,1)} %constant_dynamic-update-slice_fusion, s32[]{:T(128)S(6)} %select_n.32, bf16[512,2048]{1,0:T(8,128)(2,1)} %param.16), kind=kOutput, calls=%fused_computation.63 | convolution fusion | flops 2152725504 | bytes 11538436 | tf_op jit(solution)/shard_map/dot_general | solution.py:72
  91.1 68.2 %all-gather.7.cloned.1.call-done = bf16[2048,1536]{1,0:T(8,128)(2,1)} async-done(((bf16[512,1536]{1,0:T(8,128)(2,1)}), bf16[2048,1536]{1,0:T(8,128)(2,1)}) %all-gather.7.cloned.1.call-update) | async-done | bytes 6291472 | tf_op jit(solution)/shard_map/all_gather | solution.py:83
  159.2 6.2 %convolution_convert_fusion.2 = bf16[512,1536]{1,0:T(8,128)(2,1)S(1)} fusion(bf16[512,2048]{1,0:T(8,128)(2,1)S(1)} %multiply_convert_fusion, bf16[2048,1536]{1,0:T(8,128)(2,1)} %all-gather.7.cloned.1.call-done), kind=kOutput, calls=%fused_computation.11 | convolution fusion | flops 3222011904 | bytes 9961472 | tf_op jit(solution)/shard_map/dot_general | solution.py:81
  165.5 1.3 collective-permute-start.5
  166.8 1.5 collective-permute-start.6
  168.3 106.1 %all-gather.11.cloned.1.call-done = bf16[1536,2048]{1,0:T(8,128)(2,1)} async-done(((bf16[1536,512]{1,0:T(8,128)(2,1)}), bf16[1536,2048]{1,0:T(8,128)(2,1)}) %all-gather.11.cloned.1.call-update) | async-done | bytes 6291472 | tf_op jit(solution)/shard_map/all_gather | solution.py:99
  274.4 114.9 %all-gather.9.cloned.1.call-done = bf16[2048,1536]{1,0:T(8,128)(2,1)} async-done(((bf16[512,1536]{1,0:T(8,128)(2,1)}), bf16[2048,1536]{1,0:T(8,128)(2,1)}) %all-gather.9.cloned.1.call-update) | async-done | bytes 6291472 | tf_op jit(solution)/shard_map/all_gather | solution.py:88
  389.4 15.3 %convolution_convert_fusion = bf16[512,2048]{1,0:T(8,128)(2,1)} fusion(bf16[1536,2048]{1,0:T(8,128)(2,1)} %all-gather.11.cloned.1.call-done, bf16[512,1536]{1,0:T(8,128)(2,1)} %copy-done.5, bf16[1,1536]{1,0:T(2,128)(2,1)S(1)} %collective-permute-done.6, bf16[1,1536]{1,0:T(2,128)(2,1)S(1)} %collective-permute-done.5, f32[1536]{0:T(1024)S(1)} %get-tuple-element.8, ...), kind=kOutput, calls=%fused_computation.9 | convolution fusion | flops 6461587456 | bytes 18380800 | tf_op jit(solution)/shard_map/dot_general | solution.py:98
  404.7 29.5 %reduce-scatter.2.cloned.1.call-done = bf16[512,512]{1,0:T(8,128)(2,1)} async-done(((bf16[512,2048]{1,0:T(8,128)(2,1)}), bf16[512,512]{1,0:T(8,128)(2,1)}) %reduce-scatter.2.cloned.1.call-update) | async-done | bytes 524304 | tf_op jit(solution)/shard_map/reduce_scatter | solution.py:101
  434.2 2.0 add_convert_fusion
  (47 shorter events, 7.5 us)
Async XLA Ops:
  6.5 12.2 %copy-start = (bf16[512,256]{1,0:T(8,128)(2,1)S(1)}, bf16[512,256]{1,0:T(8,128)(2,1)}, u32[]{:S(2)}) copy-start(bf16[512,256]{1,0:T(8,128)(2,1)} %param.12) | copy-start | bytes 786436
  6.5 77.7 %all-gather.5.cloned.1.call-start = ((), (), s32[]{:S(2)}) async-start(), calls=%async_computation.1 | async-start | bytes 1310720 | tf_op jit(solution)/shard_map/all_gather | solution.py:63
  6.5 13.0 %copy-start.4 = (f32[2]{0:T(128)S(1)}, f32[2]{0:T(128)}, u32[]{:S(2)}) copy-start(f32[2]{0:T(128)} %param.15) | copy-start | bytes 28
  7.6 7.1 %collective-permute-start = (bf16[2,128,128]{2,1,0:T(8,128)(2,1)S(1)}, bf16[2,128,128]{2,1,0:T(8,128)(2,1)S(1)}, u32[]{:S(2)}, u32[]{:S(2)}) collective-permute-start(bf16[2,128,128]{2,1,0:T(8,128)(2,1)S(1)} %get-tuple-element.12), channel_id=1, source_target_pairs={{0,4},{4,8},{8,12},{1,5},{5,9},{9,13},{2,6},{6,10},{10,14},{3,7},{... | collective-permute-start | bytes 196616 | tf_op jit(solution)/shard_map/ppermute | solution.py:21
  12.6 6.2 %collective-permute-start.1 = (bf16[2,128,128]{2,1,0:T(8,128)(2,1)S(1)}, bf16[2,128,128]{2,1,0:T(8,128)(2,1)S(1)}, u32[]{:S(2)}, u32[]{:S(2)}) collective-permute-start(bf16[2,128,128]{2,1,0:T(8,128)(2,1)S(1)} %get-tuple-element.13), channel_id=1, source_target_pairs={{4,0},{8,4},{12,8},{5,1},{9,5},{13,9},{6,2},{10,6},{14,10},{7,3},{... | collective-permute-start | bytes 196616 | tf_op jit(solution)/shard_map/ppermute | solution.py:23
  22.3 2.1 copy-start.1
  22.3 136.9 %all-gather.7.cloned.1.call-start = ((), (), s32[]{:S(2)}) async-start(), calls=%async_computation.2 | async-start | bytes 7864320 | tf_op jit(solution)/shard_map/all_gather | solution.py:83
  23.1 251.4 %all-gather.11.cloned.1.call-start = ((), (), s32[]{:S(2)}) async-start(), calls=%async_computation.4 | async-start | bytes 7864320 | tf_op jit(solution)/shard_map/all_gather | solution.py:99
  23.8 365.6 %all-gather.9.cloned.1.call-start = ((), (), s32[]{:S(2)}) async-start(), calls=%async_computation.3 | async-start | bytes 7864320 | tf_op jit(solution)/shard_map/all_gather | solution.py:88
  24.4 409.9 %reduce-scatter.2.cloned.1.call-start = ((), (), s32[]{:S(2)}) async-start(), calls=%async_computation.5 | async-start | bytes 2621440 | tf_op jit(solution)/shard_map/reduce_scatter | solution.py:101
  24.4 19.9 %collective-permute-start.2 = (bf16[1024,512]{1,0:T(8,128)(2,1)S(1)}, bf16[1024,512]{1,0:T(8,128)(2,1)S(1)}, u32[]{:S(2)}, u32[]{:S(2)}) collective-permute-start(bf16[1024,512]{1,0:T(8,128)(2,1)S(1)} %copy-done.1), channel_id=1, source_target_pairs={{0,1},{1,2},{2,3},{3,0},{4,5},{5,6},{6,7},{7,4},{8,9},{9,10},{10,1... | collective-permute-start | bytes 3145736 | tf_op jit(solution)/shard_map/ppermute | solution.py:68
  44.3 14.2 %collective-permute-start.3 = (bf16[1024,512]{1,0:T(8,128)(2,1)S(1)}, bf16[1024,512]{1,0:T(8,128)(2,1)S(1)}, u32[]{:S(2)}, u32[]{:S(2)}) collective-permute-start(bf16[1024,512]{1,0:T(8,128)(2,1)S(1)} %collective-permute-done.2), channel_id=1, source_target_pairs={{0,1},{1,2},{2,3},{3,0},{4,5},{5,6},{6,7},{7,4},{8,9},{9,10},{10,1... | collective-permute-start | bytes 3145736 | tf_op jit(solution)/shard_map/ppermute | solution.py:68
  58.5 14.3 %collective-permute-start.4 = (bf16[1024,512]{1,0:T(8,128)(2,1)S(1)}, bf16[1024,512]{1,0:T(8,128)(2,1)}, u32[]{:S(2)}, u32[]{:S(2)}) collective-permute-start(bf16[1024,512]{1,0:T(8,128)(2,1)S(1)} %collective-permute-done.3), channel_id=1, source_target_pairs={{0,1},{1,2},{2,3},{3,0},{4,5},{5,6},{6,7},{7,4},{8,9},{9,10},{10,1... | collective-permute-start | bytes 3145736 | tf_op jit(solution)/shard_map/ppermute | solution.py:68
  84.3 6.1 %copy-start.3 = (f32[2048]{0:T(1024)S(1)}, f32[2048]{0:T(1024)}, u32[]{:S(2)}) copy-start(f32[2048]{0:T(1024)} %param.18) | copy-start | bytes 24580
  91.0 77.2 %copy-start.2 = (f32[3,1536]{1,0:T(4,128)S(1)}, f32[3,1536]{1,0:T(4,128)}, u32[]{:S(2)}) copy-start(f32[3,1536]{1,0:T(4,128)} %param.21) | copy-start | bytes 55300
  91.0 298.3 %copy-start.6 = (f32[1536]{0:T(1024)S(1)}, f32[1536]{0:T(1024)}, u32[]{:S(2)}) copy-start(f32[1536]{0:T(1024)} %param.22) | copy-start | bytes 18436
  165.4 2.8 copy-start.5
  165.5 223.9 %collective-permute-start.5 = (bf16[1,1536]{1,0:T(2,128)(2,1)S(1)}, bf16[1,1536]{1,0:T(2,128)(2,1)S(1)}, u32[]{:S(2)}, u32[]{:S(2)}) collective-permute-start(bf16[1,1536]{1,0:T(2,128)(2,1)S(1)} %get-tuple-element.10), channel_id=1, source_target_pairs={{0,4},{4,8},{8,12},{1,5},{5,9},{9,13},{2,6},{6,10},{10,14},{3,7},{... | collective-permute-start | bytes 9224 | tf_op jit(solution)/shard_map/ppermute | solution.py:21
  166.8 222.6 %collective-permute-start.6 = (bf16[1,1536]{1,0:T(2,128)(2,1)S(1)}, bf16[1,1536]{1,0:T(2,128)(2,1)S(1)}, u32[]{:S(2)}, u32[]{:S(2)}) collective-permute-start(bf16[1,1536]{1,0:T(2,128)(2,1)S(1)} %get-tuple-element.11), channel_id=1, source_target_pairs={{4,0},{8,4},{12,8},{5,1},{9,5},{13,9},{6,2},{10,6},{14,10},{7,3},{... | collective-permute-start | bytes 9224 | tf_op jit(solution)/shard_map/ppermute | solution.py:23
Sparse Core Ops, SparseCore 0:
  22.4 19.8 all-gather.4
  43.9 115.3 all-gather.6
  160.8 113.5 all-gather.10
  275.9 113.4 all-gather.8
  404.8 29.3 reduce-scatter.1
